TPU v7x, 32 devices: a whole 2x2x4 slice. The times are simulated.
32 devices in a mesh: rep: 4 (over z), fs: 4 (over y, x), tp: 2 (over core).
Axes of the slice: x: 2, y: 2, z: 4, core: 2. Of those that a mesh axis runs over, the one named last changes fastest.
Arguments:
- tokens_in: bfloat16 [3072, 1024], P(('rep', 'fs', 'tp')), may hold values from -6 to 6
- out_grad: bfloat16 [3072, 1024], P(('rep', 'fs', 'tp')), may hold values from -6 to 6
- gate_weight: bfloat16 [1024, 2816], P('fs', 'tp'), may hold values from -0.1875 to 0.1875
- up_weight: bfloat16 [1024, 2816], P('fs', 'tp'), may hold values from -0.1875 to 0.1875
- down_weight: bfloat16 [2816, 1024], P('tp', 'fs'), may hold values from -0.109375 to 0.109375
Outputs:
- grad_in: bfloat16 [3072, 1024], P(('rep', 'fs', 'tp'))
- grad_gate_w: float32 [1024, 2816], P('fs', 'tp')
- grad_up_w: float32 [1024, 2816], P('fs', 'tp')
- grad_down_w: float32 [2816, 1024], P('tp', 'fs')
All inputs are finite; a program needn't handle non-finite values.
Results may differ from a plain program's by a relative error of at most 0.02.
Values may be sent and summed in bfloat16 or wider, within the bound.
A program may use at most 64 MiB of HBM per device.

v0:
```python
import jax
import jax.numpy as jnp
from jax import lax
from jax.sharding import PartitionSpec as P


def contract_last(left, right):
    return lax.dot_general(
        left, right, (((1,), (1,)), ((), ())), preferred_element_type=jnp.float32
    )


def contract_first(left, right):
    return lax.dot_general(
        left, right, (((0,), (0,)), ((), ())), preferred_element_type=jnp.float32
    )


def body(tokens_in, out_grad, gate_weight, up_weight, down_weight):
    replicas = lax.axis_size("rep")
    shards = lax.axis_size("fs")
    columns = lax.axis_size("tp")
    local_rows = tokens_in.shape[0]
    hidden_cols = gate_weight.shape[1]
    factor = (local_rows * replicas * shards * columns) ** (-0.5)
    part = hidden_cols // replicas
    offset = lax.axis_index("rep") * part
    pieces = jnp.stack(
        [
            lax.dynamic_slice_in_dim(gate_weight, offset, part, 1).T,
            lax.dynamic_slice_in_dim(up_weight, offset, part, 1).T,
            lax.dynamic_slice_in_dim(down_weight, offset, part, 0),
        ]
    )
    full = lax.all_gather(pieces, "fs", axis=2, tiled=True)
    gate_full, up_full, down_full = (full[0], full[1], full[2])
    both = lax.all_gather(jnp.stack([tokens_in, out_grad]), ("rep", "tp"), axis=1, tiled=True)
    tokens_all, grads_all = (both[0], both[1])
    gate = contract_last(tokens_all, gate_full).astype(jnp.bfloat16)
    up_proj = contract_last(tokens_all, up_full).astype(jnp.bfloat16)
    gate_wide = gate.astype(jnp.float32)
    up_wide = up_proj.astype(jnp.float32)
    sigmoid = jax.nn.sigmoid(gate_wide)
    activated = gate_wide * sigmoid
    hidden = (activated * up_wide).astype(jnp.bfloat16)
    grad_hidden = contract_last(grads_all, down_full).astype(jnp.bfloat16)
    grad_wide = grad_hidden.astype(jnp.float32)
    grad_gate = (grad_wide * up_wide * sigmoid * (1.0 + gate_wide * (1.0 - sigmoid))).astype(
        jnp.bfloat16
    )
    grad_up = (grad_wide * activated).astype(jnp.bfloat16)
    weights = factor * jnp.stack(
        [
            contract_first(grad_gate, tokens_all),
            contract_first(grad_up, tokens_all),
            contract_first(hidden, grads_all),
        ]
    )
    owned = lax.psum_scatter(weights.astype(jnp.bfloat16), "fs", scatter_dimension=2, tiled=True)
    summed = lax.all_gather(owned, "rep", axis=1, tiled=True).astype(jnp.float32)
    partial = jnp.dot(grad_gate, gate_full, preferred_element_type=jnp.float32) + jnp.dot(
        grad_up, up_full, preferred_element_type=jnp.float32
    )
    grad_in = lax.psum_scatter(
        partial.astype(jnp.bfloat16), ("rep", "tp"), scatter_dimension=0, tiled=True
    )
    return (grad_in, summed[0].T, summed[1].T, summed[2])


def solution(mesh):
    placed = (
        P(("rep", "fs", "tp"), None),
        P(("rep", "fs", "tp"), None),
        P("fs", "tp"),
        P("fs", "tp"),
        P("tp", "fs"),
    )
    return jax.shard_map(
        body,
        mesh=mesh,
        in_specs=placed,
        out_specs=(P(("rep", "fs", "tp"), None), P("fs", "tp"), P("fs", "tp"), P("tp", "fs")),
        check_vma=False,
    )
```

profile of v0, /device:TPU:0, one launch (start us, length us, event | category | flops | bytes accessed | tf_op | source)
XLA Modules:
  0.0 225.2 jit_solution(11727370553388090820)
XLA Ops:
  7.2 0.0 copy-start
  7.2 0.0 all-gather.6.cloned.1.call-start
  7.2 1.0 copy-done
  8.3 0.0 copy-start.1
  8.3 0.0 copy-start.2
  8.3 1.3 constant_dynamic-slice_fusion
  9.6 0.1 copy.16
  9.8 0.1 copy.15
  9.9 0.9 pad_maximum_fusion
  10.8 0.0 all-gather.6.cloned.1.call-update
  10.8 0.0 all-gather.4.cloned.1.call-start
  10.8 0.0 copy-done.1
  10.8 0.0 copy-done.2
  10.9 0.8 pad_maximum_fusion.1
  11.6 0.0 all-gather.4.cloned.1.call-update
  11.7 0.0 reduce-scatter.5.cloned.1.call-start
  11.7 37.5 %all-gather.6.cloned.1.call-done = bf16[3,352,1024]{2,1,0:T(8,128)(2,1)} async-done(((bf16[3,352,256]{2,1,0:T(8,128)(2,1)}), bf16[3,352,1024]{2,1,0:T(8,128)(2,1)}) %all-gather.6.cloned.1.call-update) | async-done | bytes 2162704 | tf_op jit(solution)/shard_map/all_gather | solution.py:35
  49.2 40.4 %all-gather.4.cloned.1.call-done = bf16[2,768,1024]{2,1,0:T(8,128)(2,1)} async-done(((bf16[2,96,1024]{2,1,0:T(8,128)(2,1)}), bf16[2,768,1024]{2,1,0:T(8,128)(2,1)}) %all-gather.4.cloned.1.call-update) | async-done | bytes 3145744 | tf_op jit(solution)/shard_map/all_gather | solution.py:37
  89.7 0.0 copy-start.3
  89.7 2.5 %convolution_convert_fusion.1 = bf16[768,352]{0,1:T(8,128)(2,1)S(1)} fusion(bf16[2,768,1024]{2,1,0:T(8,128)(2,1)} %all-gather.4.cloned.1.call-done, bf16[3,352,1024]{2,1,0:T(8,128)(2,1)} %all-gather.6.cloned.1.call-done), kind=kOutput, calls=%fused_computation.20 | convolution fusion | flops 553918464 | bytes 2834432 | tf_op jit(solution)/shard_map/dot_general | solution.py:8
  92.2 0.1 copy-done.3
  92.2 0.0 copy-start.7
  92.3 2.2 fusion.2
  94.4 0.0 copy-done.4
  94.4 0.8 convolution_convert_fusion
  95.2 0.0 copy-start.5
  95.2 0.8 convolution_bitcast_fusion
  96.1 0.9 convolution_bitcast_fusion.1
  96.9 0.0 copy-done.7
  96.9 0.0 copy-done.5
  96.9 1.0 convolution_bitcast_fusion.2
  98.0 2.0 fusion
  99.9 0.0 reduce-scatter.5.cloned.1.call-update
  100.0 0.0 all-gather.8.cloned.1.call-start
  100.0 34.8 %reduce-scatter.5.cloned.1.call-done = bf16[3,352,256]{2,1,0:T(8,128)(2,1)} async-done(((bf16[3,352,1024]{2,1,0:T(8,128)(2,1)}), bf16[3,352,256]{2,1,0:T(8,128)(2,1)}) %reduce-scatter.5.cloned.1.call-update) | async-done | bytes 540688 | tf_op jit(solution)/shard_map/reduce_scatter | solution.py:59
  134.8 0.0 all-gather.8.cloned.1.call-update
  134.8 0.0 reduce-scatter.3.cloned.1.call-start
  134.8 0.0 copy-start.6
  134.8 2.5 %fusion.12 = f32[768,1024]{1,0:T(8,128)S(1)} fusion(bf16[3,352,1024]{2,1,0:T(8,128)(2,1)S(1)} %copy-done.4, bf16[768,352]{0,1:T(8,128)(2,1)} %copy-done.7, bf16[768,352]{0,1:T(8,128)(2,1)S(1)} %fusion.2, bf16[768,352]{0,1:T(8,128)(2,1)} %copy-done.5), kind=kOutput, calls=%fused_computation.33 | convolution fusion | flops 557162496 | bytes 5488640 | tf_op jit(solution)/shard_map/dot_general | solution.py:61
  137.4 0.0 copy-done.6
  137.4 2.3 %add_convert_fusion = bf16[768,1024]{1,0:T(8,128)(2,1)} fusion(f32[768,1024]{1,0:T(8,128)S(1)} %fusion.12, bf16[3,352,1024]{2,1,0:T(8,128)(2,1)S(1)} %copy-done.4, bf16[768,352]{0,1:T(8,128)(2,1)S(1)} %fusion.2, bf16[768,352]{0,1:T(8,128)(2,1)S(1)} %copy-done.6), kind=kOutput, calls=%fused_computation.2 | convolution fusion | flops 557383680 | bytes 6520832 | tf_op jit(solution)/shard_map/dot_general | solution.py:61
  139.7 0.0 reduce-scatter.3.cloned.1.call-update
  139.7 43.2 %all-gather.8.cloned.1.call-done = bf16[3,1408,256]{2,1,0:T(8,128)(2,1)} async-done(((bf16[3,352,256]{2,1,0:T(8,128)(2,1)}), bf16[3,1408,256]{2,1,0:T(8,128)(2,1)}) %all-gather.8.cloned.1.call-update) | async-done | bytes 2162704 | tf_op jit(solution)/shard_map/all_gather | solution.py:60
  183.0 2.0 convert_element_type.47
  185.0 2.0 slice_bitcast_fusion.2
  186.9 2.9 %copy.13 = f32[256,1408]{1,0:T(8,128)} copy(f32[256,1408]{0,1:T(8,128)} %get-tuple-element.14) | data formatting | bytes 2883584
  189.8 1.5 copy.14
  191.4 27.3 %reduce-scatter.3.cloned.1.call-done = bf16[96,1024]{1,0:T(8,128)(2,1)} async-done(((bf16[768,1024]{1,0:T(8,128)(2,1)}), bf16[96,1024]{1,0:T(8,128)(2,1)}) %reduce-scatter.3.cloned.1.call-update) | async-done | bytes 196624 | tf_op jit(solution)/shard_map/reduce_scatter | solution.py:64
  (2 shorter events, 0.0 us)
Async XLA Ops:
  7.2 1.1 copy-start
  7.2 42.1 %all-gather.6.cloned.1.call-start = ((), (), s32[]{:S(2)}) async-start(), calls=%async_computation.3 | async-start | bytes 2703360 | tf_op jit(solution)/shard_map/all_gather | solution.py:35
  8.3 2.5 %copy-start.1 = (bf16[96,1024]{1,0:T(8,128)(2,1)S(1)}, bf16[96,1024]{1,0:T(8,128)(2,1)}, u32[]{:S(2)}) copy-start(bf16[96,1024]{1,0:T(8,128)(2,1)} %param.6) | copy-start | bytes 589828
  8.3 2.5 %copy-start.2 = (bf16[96,1024]{1,0:T(8,128)(2,1)S(1)}, bf16[96,1024]{1,0:T(8,128)(2,1)}, u32[]{:S(2)}) copy-start(bf16[96,1024]{1,0:T(8,128)(2,1)} %param.5) | copy-start | bytes 589828
  10.8 78.9 %all-gather.4.cloned.1.call-start = ((), (), s32[]{:S(2)}) async-start(), calls=%async_computation.2 | async-start | bytes 3538944 | tf_op jit(solution)/shard_map/all_gather | solution.py:37
  11.7 123.1 %reduce-scatter.5.cloned.1.call-start = ((), (), s32[]{:S(2)}) async-start(), calls=%async_computation.5 | async-start | bytes 2703360 | tf_op jit(solution)/shard_map/reduce_scatter | solution.py:59
  89.7 2.6 %copy-start.3 = (bf16[2,768,1024]{2,1,0:T(8,128)(2,1)S(1)}, bf16[2,768,1024]{2,1,0:T(8,128)(2,1)}, u32[]{:S(2)}) copy-start(bf16[2,768,1024]{2,1,0:T(8,128)(2,1)} %all-gather.4.cloned.1.call-done) | copy-start | bytes 9437188
  92.2 4.7 %copy-start.7 = (bf16[768,352]{0,1:T(8,128)(2,1)}, bf16[768,352]{0,1:T(8,128)(2,1)S(1)}, u32[]{:S(2)}) copy-start(bf16[768,352]{0,1:T(8,128)(2,1)S(1)} %convolution_convert_fusion.1) | copy-start | bytes 1622020
  92.2 2.2 copy-start.4
  95.2 1.7 copy-start.5
  100.0 83.0 %all-gather.8.cloned.1.call-start = ((), (), s32[]{:S(2)}) async-start(), calls=%async_computation.6 | async-start | bytes 2703360 | tf_op jit(solution)/shard_map/all_gather | solution.py:60
  134.8 83.8 %reduce-scatter.3.cloned.1.call-start = ((), (), s32[]{:S(2)}) async-start(), calls=%async_computation.4 | async-start | bytes 1769472 | tf_op jit(solution)/shard_map/reduce_scatter | solution.py:64
  134.8 2.6 %copy-start.6 = (bf16[768,352]{0,1:T(8,128)(2,1)S(1)}, bf16[768,352]{0,1:T(8,128)(2,1)}, u32[]{:S(2)}) copy-start(bf16[768,352]{0,1:T(8,128)(2,1)} %copy-done.5) | copy-start | bytes 1622020
Sparse Core Ops, SparseCore 0:
  10.9 38.2 all-gather.5
  51.4 38.1 all-gather.3
  100.1 34.6 reduce-scatter.4
  136.2 46.7 all-gather.7
  185.7 32.8 reduce-scatter.2
where the time goes:
time: 225 us
  waiting for transfers between devices  183 us (81%)
  between operations  13.9 us (6%)
  matrix products  13 us (6%)
  local copies, waits for them, and re-layouts  9.14 us (4%)
  other arithmetic  5.58 us (2%)
    all_gather x1, waiting for transfers between devices, body(): lax.all_gather(owned, 'rep', axis=1, tiled=True).astype(jnp.float32)  43.2 us
    all_gather x1, waiting for transfers between devices, body(): lax.all_gather(jnp.stack([tokens_in, out_grad]), ('rep', 'tp'), axis=1, t...  40.4 us
    all_gather x1, waiting for transfers between devices, body(): full = lax.all_gather(pieces, 'fs', axis=2, tiled=True)  37.5 us
    reduce_scatter x1, waiting for transfers between devices, body(): lax.psum_scatter(weights.astype(jnp.bfloat16), 'fs', scatter_dimension=2,...  34.8 us
    reduce_scatter x1, waiting for transfers between devices, body(): lax.psum_scatter(partial.astype(jnp.bfloat16), ('rep', 'tp'), scatter_dim...  27.3 us
    unnamed x20, local copies, waits for them, and re-layouts  5.87 us
    dot_general x3, matrix products, contract_last(): lax.dot_general(left, right, (((1,), (1,)), ((), ())), preferred_element_...  5.44 us
  transfers between devices with their start and end apart: 5, of which 5 were waited for; matrix products, arithmetic and copies ran while one was open for 6% of the time, Pallas kernels for 0%

commit v1 on v0

--- a/solution.py
+++ b/solution.py
@@ -32,7 +32,12 @@
             lax.dynamic_slice_in_dim(down_weight, offset, part, 0),
         ]
     )
-    full = lax.all_gather(pieces, "fs", axis=2, tiled=True)
+    ring = [pieces]
+    for hop in range(3):
+        ring.append(lax.ppermute(ring[-1], "fs", [(dev, (dev + 1) % 4) for dev in range(4)]))
+    full = jnp.roll(
+        jnp.concatenate(ring[::-1], axis=2), (lax.axis_index("fs") + 1) * ring[0].shape[2], axis=2
+    )
     gate_full, up_full, down_full = (full[0], full[1], full[2])
     both = lax.all_gather(jnp.stack([tokens_in, out_grad]), ("rep", "tp"), axis=1, tiled=True)
     tokens_all, grads_all = (both[0], both[1])

time: 225 us -> 200 us (0.89)
  waiting for transfers between devices: 183 us -> 146 us
  local copies, waits for them, and re-layouts: 9.14 us -> 13.3 us
  starting transfers between devices: 0.2 us -> 3.96 us
    ppermute x0 -> x3, waiting for transfers between devices: none -> 40.6 us  [body(): lax.ppermute(ring[-1], 'fs', [(dev, (dev + 1) % 4) for dev in range(4)])]
    all_gather x1, waiting for transfers between devices: 40.4 us -> 0.01 us  [body(): lax.all_gather(jnp.stack([tokens_in, out_grad]), ('rep', 'tp'), axis=1, t...]
    all_gather x1 -> x0, waiting for transfers between devices: 37.5 us -> none  [body(): full = lax.all_gather(pieces, 'fs', axis=2, tiled=True)]
    unnamed x20 -> x14, local copies, waits for them, and re-layouts: 5.87 us -> 10 us
    ppermute x0 -> x3, starting transfers between devices: none -> 3.81 us  [body(): lax.ppermute(ring[-1], 'fs', [(dev, (dev + 1) % 4) for dev in range(4)])]
  transfers between devices with their start and end apart: 5 -> 7, of which waited for: 5 -> 6; matrix products, arithmetic and copies ran while one was open for 6% -> 11% of each run, Pallas kernels for 0% -> 0%
where the time goes in v1:
time: 200 us
  waiting for transfers between devices  146 us (73%)
  matrix products  14.8 us (7%)
  between operations  13.9 us (7%)
  local copies, waits for them, and re-layouts  13.3 us (7%)
  other arithmetic  7.64 us (4%)
  starting transfers between devices  3.96 us (2%)
    all_gather x1, waiting for transfers between devices, body(): lax.all_gather(owned, 'rep', axis=1, tiled=True).astype(jnp.float32)  42.4 us
    ppermute x3, waiting for transfers between devices, body(): lax.ppermute(ring[-1], 'fs', [(dev, (dev + 1) % 4) for dev in range(4)])  40.6 us
    reduce_scatter x1, waiting for transfers between devices, body(): lax.psum_scatter(weights.astype(jnp.bfloat16), 'fs', scatter_dimension=2,...  35.7 us
    reduce_scatter x1, waiting for transfers between devices, body(): lax.psum_scatter(partial.astype(jnp.bfloat16), ('rep', 'tp'), scatter_dim...  27.3 us
    unnamed x14, local copies, waits for them, and re-layouts  10 us
    dot_general x3, matrix products, contract_last(): lax.dot_general(left, right, (((1,), (1,)), ((), ())), preferred_element_...  6.31 us
  transfers between devices with their start and end apart: 7, of which 6 were waited for; matrix products, arithmetic and copies ran while one was open for 11% of the time, Pallas kernels for 0%

profile of v1, /device:TPU:0, one launch (start us, length us, event | category | flops | bytes accessed | tf_op | source)
XLA Modules:
  0.0 199.7 jit_solution(2071983631328511997)
XLA Ops:
  7.2 0.0 copy-start
  7.2 0.0 all-gather.3.cloned.1.call-start
  7.2 1.9 pad_maximum_fusion.1
  9.1 0.0 all-gather.3.cloned.1.call-update
  9.1 0.0 reduce-scatter.5.cloned.1.call-start
  9.2 1.2 constant_dynamic-slice_fusion
  10.4 0.1 copy.16
  10.6 0.1 copy.15
  10.7 0.0 copy-done
  10.7 0.1 pad_maximum_fusion
  10.8 3.0 %collective-permute-start = (bf16[3,352,256]{2,1,0:T(8,128)(2,1)S(1)}, bf16[3,352,256]{2,1,0:T(8,128)(2,1)S(1)}, u32[]{:S(2)}, u32[]{:S(2)}) collective-permute-start(bf16[3,352,256]{2,1,0:T(8,128)(2,1)S(1)} %pad_maximum_fusion), channel_id=1, source_target_pairs={{0,2},{2,4},{4,6},{6,0},{1,3},{3,5},{5,7},{7,1},{8,10},{10,12},{12... | collective-permute-start | bytes 1622024 | tf_op jit(solution)/shard_map/ppermute | solution.py:37
  13.8 13.2 %collective-permute-done = bf16[3,352,256]{2,1,0:T(8,128)(2,1)S(1)} collective-permute-done((bf16[3,352,256]{2,1,0:T(8,128)(2,1)S(1)}, bf16[3,352,256]{2,1,0:T(8,128)(2,1)S(1)}, u32[]{:S(2)}, u32[]{:S(2)}) %collective-permute-start) | collective-permute-done | bytes 540704 | tf_op jit(solution)/shard_map/ppermute | solution.py:37
  27.1 0.8 collective-permute-start.1
  27.8 13.7 %collective-permute-done.1 = bf16[3,352,256]{2,1,0:T(8,128)(2,1)S(1)} collective-permute-done((bf16[3,352,256]{2,1,0:T(8,128)(2,1)S(1)}, bf16[3,352,256]{2,1,0:T(8,128)(2,1)S(1)}, u32[]{:S(2)}, u32[]{:S(2)}) %collective-permute-start.1) | collective-permute-done | bytes 540704 | tf_op jit(solution)/shard_map/ppermute | solution.py:37
  41.5 0.0 collective-permute-start.2
  41.5 13.7 %collective-permute-done.2 = bf16[3,352,256]{2,1,0:T(8,128)(2,1)S(1)} collective-permute-done((bf16[3,352,256]{2,1,0:T(8,128)(2,1)S(1)}, bf16[3,352,256]{2,1,0:T(8,128)(2,1)S(1)}, u32[]{:S(2)}, u32[]{:S(2)}) %collective-permute-start.2) | collective-permute-done | bytes 540704 | tf_op jit(solution)/shard_map/ppermute | solution.py:37
  55.2 0.9 constant_dynamic-update-slice_fusion.7
  56.1 0.9 constant_dynamic-update-slice_fusion.6
  57.0 0.9 constant_dynamic-update-slice_fusion.5
  57.9 0.9 constant_dynamic-update-slice_fusion.4
  58.7 0.9 constant_dynamic-update-slice_fusion.3
  59.6 0.9 constant_dynamic-update-slice_fusion.2
  60.5 0.9 constant_dynamic-update-slice_fusion.1
  61.3 0.9 constant_dynamic-update-slice_fusion
  62.2 0.0 all-gather.3.cloned.1.call-done
  62.2 0.0 copy-start.1
  62.2 2.5 %convolution_convert_fusion = bf16[768,352]{0,1:T(8,128)(2,1)S(1)} fusion(bf16[2,768,1024]{2,1,0:T(8,128)(2,1)} %all-gather.3.cloned.1.call-done, bf16[3,352,2048]{2,1,0:T(8,128)(2,1)} %constant_dynamic-update-slice_fusion, s32[]{:T(128)S(6)} %select_n.20), kind=kOutput, calls=%fused_computation.19 | convolution fusion | flops 553918464 | bytes 2834436 | tf_op jit(solution)/shard_map/dot_general | solution.py:8
  64.7 0.1 copy-done.1
  64.8 1.9 fusion.2
  66.7 1.9 convolution_convert_fusion.1
  68.6 0.8 convolution_bitcast_fusion
  69.5 0.9 convolution_bitcast_fusion.1
  70.3 1.0 convolution_bitcast_fusion.2
  71.4 2.0 fusion
  73.3 0.0 reduce-scatter.5.cloned.1.call-update
  73.4 0.0 all-gather.5.cloned.1.call-start
  73.4 35.7 %reduce-scatter.5.cloned.1.call-done = bf16[3,352,256]{2,1,0:T(8,128)(2,1)} async-done(((bf16[3,352,1024]{2,1,0:T(8,128)(2,1)}), bf16[3,352,256]{2,1,0:T(8,128)(2,1)}) %reduce-scatter.5.cloned.1.call-update) | async-done | bytes 540688 | tf_op jit(solution)/shard_map/reduce_scatter | solution.py:64
  109.1 0.0 all-gather.5.cloned.1.call-update
  109.2 0.0 reduce-scatter.3.cloned.1.call-start
  109.2 2.2 %fusion.12 = f32[768,1024]{1,0:T(8,128)S(1)} fusion(bf16[3,352,2048]{2,1,0:T(8,128)(2,1)} %constant_dynamic-update-slice_fusion, s32[]{:T(128)S(6)} %add.39, s32[]{:T(128)S(6)} %select_n.20, bf16[768,352]{0,1:T(8,128)(2,1)S(1)} %fusion.2, bf16[768,352]{0,1:T(8,128)(2,1)S(1)} %convolution_convert_fusion), kind=kOutput, calls=%fused_computation.33 | convolution fusion | flops 555810816 | bytes 4947976 | tf_op jit(solution)/shard_map/dot_general | solution.py:66
  111.4 3.6 %add_convert_fusion = bf16[768,1024]{1,0:T(8,128)(2,1)} fusion(f32[768,1024]{1,0:T(8,128)S(1)} %fusion.12, bf16[3,352,2048]{2,1,0:T(8,128)(2,1)} %constant_dynamic-update-slice_fusion, s32[]{:T(128)S(6)} %select_n.20, bf16[768,352]{0,1:T(8,128)(2,1)S(1)} %convolution_convert_fusion.1, bf16[768,352]{0,1:T(8,128)(2,1)S(1)} %fusion.2, ...), kind=kOutput, calls=%fused_computation.2 | convolution fusion | flops 558735360 | bytes 7061508 | tf_op jit(solution)/shard_map/dot_general | solution.py:66
  115.0 0.0 reduce-scatter.3.cloned.1.call-update
  115.0 42.4 %all-gather.5.cloned.1.call-done = bf16[3,1408,256]{2,1,0:T(8,128)(2,1)} async-done(((bf16[3,352,256]{2,1,0:T(8,128)(2,1)}), bf16[3,1408,256]{2,1,0:T(8,128)(2,1)}) %all-gather.5.cloned.1.call-update) | async-done | bytes 2162704 | tf_op jit(solution)/shard_map/all_gather | solution.py:65
  157.5 2.0 convert_element_type.47
  159.4 2.0 slice_bitcast_fusion.2
  161.4 2.9 %copy.13 = f32[256,1408]{1,0:T(8,128)} copy(f32[256,1408]{0,1:T(8,128)} %get-tuple-element.14) | data formatting | bytes 2883584
  164.3 1.5 copy.14
  165.9 27.3 %reduce-scatter.3.cloned.1.call-done = bf16[96,1024]{1,0:T(8,128)(2,1)} async-done(((bf16[768,1024]{1,0:T(8,128)(2,1)}), bf16[96,1024]{1,0:T(8,128)(2,1)}) %reduce-scatter.3.cloned.1.call-update) | async-done | bytes 196624 | tf_op jit(solution)/shard_map/reduce_scatter | solution.py:69
  (1 shorter events, 0.0 us)
Async XLA Ops:
  7.2 3.5 %copy-start = (bf16[1408,256]{1,0:T(8,128)(2,1)S(1)}, bf16[1408,256]{1,0:T(8,128)(2,1)}, u32[]{:S(2)}) copy-start(bf16[1408,256]{1,0:T(8,128)(2,1)} %param.9) | copy-start | bytes 2162692
  7.2 55.0 %all-gather.3.cloned.1.call-start = ((), (), s32[]{:S(2)}) async-start(), calls=%async_computation.2 | async-start | bytes 3538944 | tf_op jit(solution)/shard_map/all_gather | solution.py:42
  9.1 100.0 %reduce-scatter.5.cloned.1.call-start = ((), (), s32[]{:S(2)}) async-start(), calls=%async_computation.4 | async-start | bytes 2703360 | tf_op jit(solution)/shard_map/reduce_scatter | solution.py:64
  10.8 16.2 %collective-permute-start = (bf16[3,352,256]{2,1,0:T(8,128)(2,1)S(1)}, bf16[3,352,256]{2,1,0:T(8,128)(2,1)S(1)}, u32[]{:S(2)}, u32[]{:S(2)}) collective-permute-start(bf16[3,352,256]{2,1,0:T(8,128)(2,1)S(1)} %pad_maximum_fusion), channel_id=1, source_target_pairs={{0,2},{2,4},{4,6},{6,0},{1,3},{3,5},{5,7},{7,1},{8,10},{10,12},{12... | collective-permute-start | bytes 1622024 | tf_op jit(solution)/shard_map/ppermute | solution.py:37
  27.1 14.4 %collective-permute-start.1 = (bf16[3,352,256]{2,1,0:T(8,128)(2,1)S(1)}, bf16[3,352,256]{2,1,0:T(8,128)(2,1)S(1)}, u32[]{:S(2)}, u32[]{:S(2)}) collective-permute-start(bf16[3,352,256]{2,1,0:T(8,128)(2,1)S(1)} %collective-permute-done), channel_id=1, source_target_pairs={{0,2},{2,4},{4,6},{6,0},{1,3},{3,5},{5,7},{7,1},{8,10},{10,12},{12... | collective-permute-start | bytes 1622024 | tf_op jit(solution)/shard_map/ppermute | solution.py:37
  41.5 13.7 %collective-permute-start.2 = (bf16[3,352,256]{2,1,0:T(8,128)(2,1)S(1)}, bf16[3,352,256]{2,1,0:T(8,128)(2,1)S(1)}, u32[]{:S(2)}, u32[]{:S(2)}) collective-permute-start(bf16[3,352,256]{2,1,0:T(8,128)(2,1)S(1)} %collective-permute-done.1), channel_id=1, source_target_pairs={{0,2},{2,4},{4,6},{6,0},{1,3},{3,5},{5,7},{7,1},{8,10},{10,12},{12... | collective-permute-start | bytes 1622024 | tf_op jit(solution)/shard_map/ppermute | solution.py:37
  62.2 2.6 %copy-start.1 = (bf16[2,768,1024]{2,1,0:T(8,128)(2,1)S(1)}, bf16[2,768,1024]{2,1,0:T(8,128)(2,1)}, u32[]{:S(2)}) copy-start(bf16[2,768,1024]{2,1,0:T(8,128)(2,1)} %all-gather.3.cloned.1.call-done) | copy-start | bytes 9437188
  73.4 84.1 %all-gather.5.cloned.1.call-start = ((), (), s32[]{:S(2)}) async-start(), calls=%async_computation.5 | async-start | bytes 2703360 | tf_op jit(solution)/shard_map/all_gather | solution.py:65
  109.2 84.0 %reduce-scatter.3.cloned.1.call-start = ((), (), s32[]{:S(2)}) async-start(), calls=%async_computation.3 | async-start | bytes 1769472 | tf_op jit(solution)/shard_map/reduce_scatter | solution.py:69
Sparse Core Ops, SparseCore 0:
  10.2 40.9 all-gather.2
  73.5 35.5 reduce-scatter.4
  110.7 46.7 all-gather.4
  160.2 32.9 reduce-scatter.2
